TPU v7x, 128 devices: a whole 4x4x4 slice. The times are simulated.
128 devices in a mesh: rep: 2 (over x_hi), fs: 16 (over y, x_lo, core), tp: 4 (over z).
Axes of the slice: x: 4 (x_hi: 2, x_lo: 2; x = x_hi * 2 + x_lo), y: 4, z: 4, core: 2. Of those that a mesh axis runs over, the one named last changes fastest.
Arguments:
- tokens: bfloat16 [16384, 2048], P(('rep', 'fs', 'tp')), may hold values from -3 to 3
- mixer_output: bfloat16 [16384, 2048], P(('rep', 'fs', 'tp')), may hold values from -6 to 6
- early_norm: float32 [2048], replicated, may hold values from 0.75 to 1.25
- early_gate: bfloat16 [2048, 5120], P('fs', 'tp'), may hold values from -0.125 to 0.125
- early_value: bfloat16 [2048, 5120], P('fs', 'tp'), may hold values from -0.125 to 0.125
- early_down: bfloat16 [5120, 2048], P('tp', 'fs'), may hold values from -0.078125 to 0.078125
- early_post: float32 [2048], replicated, may hold values from 0.75 to 1.25
- mixer_gain: float32 [2048], replicated, may hold values from 0.75 to 1.25
- later_norm: float32 [2048], replicated, may hold values from 0.75 to 1.25
- later_gate: bfloat16 [2048, 5120], P('fs', 'tp'), may hold values from -0.125 to 0.125
- later_value: bfloat16 [2048, 5120], P('fs', 'tp'), may hold values from -0.125 to 0.125
- later_down: bfloat16 [5120, 2048], P('tp', 'fs'), may hold values from -0.078125 to 0.078125
- later_post: float32 [2048], replicated, may hold values from 0.75 to 1.25
Outputs:
- layer_out: bfloat16 [16384, 2048], P(('rep', 'fs', 'tp'))
All inputs are finite; a program needn't handle non-finite values.
Results may differ from a plain program's by a relative error of at most 0.015.
Values may be sent and summed in bfloat16 or wider, within the bound.
A program may use at most 128 MiB of HBM per device.

v0:
```python
import jax
import jax.numpy as jnp
from jax import lax
from jax.sharding import PartitionSpec as P

epsilon = 1e-06


def over_all(piece, axis, dim, step, start):

    def gathered(part):
        return lax.all_gather(part, axis, axis=dim, tiled=True)

    return step(start, jax.tree.map(gathered, piece), jnp.int32(0))


def own_rows(product, extent, axis):
    everything = product(jnp.int32(0), lax.axis_size(axis) * extent)
    own = lax.psum_scatter(everything.astype(jnp.bfloat16), axis, scatter_dimension=0, tiled=True)
    return own.astype(jnp.float32)


def rms_scale(values, gain):
    values = values.astype(jnp.float32)
    scale = lax.rsqrt(jnp.mean(values * values, axis=-1, keepdims=True) + epsilon)
    return values * scale * gain


def half_branch(normed, gate_piece, value_piece, down_piece):
    all_rows = lax.all_gather(normed, "tp", axis=0, tiled=True)
    empty = jnp.zeros((all_rows.shape[0], gate_piece.shape[1]), jnp.float32)

    def add_rows(totals, pieces, start):
        columns = lax.dynamic_slice_in_dim(all_rows, start, pieces[0].shape[0], 1)
        gate_part = jnp.dot(columns, pieces[0], preferred_element_type=jnp.float32)
        value_part = jnp.dot(columns, pieces[1], preferred_element_type=jnp.float32)
        return (totals[0] + gate_part, totals[1] + value_part)

    gate_sum, value_sum = over_all((gate_piece, value_piece), "fs", 0, add_rows, (empty, empty))
    down_block = lax.all_gather(down_piece, "fs", axis=1, tiled=True)
    hidden = (jax.nn.silu(gate_sum) * value_sum).astype(jnp.bfloat16)

    def row_term(start, count):
        rows = lax.dynamic_slice_in_dim(hidden, start, count, 0)
        return jnp.dot(rows, down_block, preferred_element_type=jnp.float32)

    return own_rows(row_term, normed.shape[0], "tp")


def on_device(
    tokens,
    mixer_output,
    early_norm,
    early_gate,
    early_value,
    early_down,
    early_post,
    mixer_gain,
    later_norm,
    later_gate,
    later_value,
    later_down,
    later_post,
):
    early_in = rms_scale(tokens, early_norm).astype(jnp.bfloat16)
    early_branch = half_branch(early_in, early_gate, early_value, early_down)
    mixed = (
        tokens.astype(jnp.float32)
        + 0.5 * rms_scale(early_branch, early_post)
        + rms_scale(mixer_output, mixer_gain)
    )
    mixed = mixed.astype(jnp.bfloat16)
    later_in = rms_scale(mixed, later_norm).astype(jnp.bfloat16)
    later_branch = half_branch(later_in, later_gate, later_value, later_down)
    layer_out = mixed.astype(jnp.float32) + 0.5 * rms_scale(later_branch, later_post)
    return layer_out.astype(jnp.bfloat16)


def solution(mesh):
    placed = (
        P(("rep", "fs", "tp"), None),
        P(("rep", "fs", "tp"), None),
        P(),
        P("fs", "tp"),
        P("fs", "tp"),
        P("tp", "fs"),
        P(),
        P(),
        P(),
        P("fs", "tp"),
        P("fs", "tp"),
        P("tp", "fs"),
        P(),
    )
    return jax.shard_map(
        on_device,
        mesh=mesh,
        in_specs=placed,
        out_specs=P(("rep", "fs", "tp"), None),
        check_vma=False,
    )
```

profile of v0, /device:TPU:1, one launch (start us, length us, event | category | flops | bytes accessed | tf_op | source)
XLA Modules:
  0.0 438.2 jit_solution(11551723246681318497)
XLA Ops:
  6.5 0.0 all-gather.9.cloned.1.call-start
  6.5 1.2 fusion.12
  7.8 2.0 fusion.14
  9.8 0.0 all-gather.9.cloned.1.call-update
  9.8 0.0 all-gather.11.cloned.1.call-start
  9.9 0.7 all-gather.11.cloned.1.call-update
  10.6 0.0 all-gather.13.cloned.1.call-start
  10.6 0.7 all-gather.13.cloned.1.call-update
  11.3 0.0 all-gather.15.cloned.1.call-start
  11.4 0.5 all-gather.15.cloned.1.call-update
  11.9 0.0 reduce-scatter.3.cloned.1.call-start
  11.9 32.1 %all-gather.9.cloned.1.call-done = bf16[512,2048]{1,0:T(8,128)(2,1)} async-done(((bf16[128,2048]{1,0:T(8,128)(2,1)}), bf16[512,2048]{1,0:T(8,128)(2,1)}) %all-gather.9.cloned.1.call-update) | async-done | bytes 2097168 | tf_op jit(solution)/shard_map/all_gather | solution.py:30
  44.0 0.0 copy-start.6
  44.0 41.1 %all-gather.11.cloned.1.call-done = bf16[2048,1280]{1,0:T(8,128)(2,1)} async-done(((bf16[128,1280]{1,0:T(8,128)(2,1)}), bf16[2048,1280]{1,0:T(8,128)(2,1)}) %all-gather.11.cloned.1.call-update) | async-done | bytes 5242896 | tf_op jit(solution)/shard_map/all_gather | solution.py:12
  85.1 7.5 %fusion.22 = f32[512,1280]{1,0:T(8,128)} fusion(bf16[512,2048]{1,0:T(8,128)(2,1)} %all-gather.9.cloned.1.call-done, bf16[2048,1280]{1,0:T(8,128)(2,1)} %all-gather.11.cloned.1.call-done), kind=kOutput, calls=%fused_computation.42 | convolution fusion | flops 2684354560 | bytes 9961472 | tf_op jit(solution)/shard_map/dot_general | solution.py:35
  92.6 33.7 %all-gather.13.cloned.1.call-done = bf16[2048,1280]{1,0:T(8,128)(2,1)} async-done(((bf16[128,1280]{1,0:T(8,128)(2,1)}), bf16[2048,1280]{1,0:T(8,128)(2,1)}) %all-gather.13.cloned.1.call-update) | async-done | bytes 5242896 | tf_op jit(solution)/shard_map/all_gather | solution.py:12
  126.3 51.5 %all-gather.15.cloned.1.call-done = bf16[1280,2048]{1,0:T(8,128)(2,1)} async-done(((bf16[1280,128]{1,0:T(8,128)(2,1)}), bf16[1280,2048]{1,0:T(8,128)(2,1)}) %all-gather.15.cloned.1.call-update) | async-done | bytes 5242896 | tf_op jit(solution)/shard_map/all_gather | solution.py:40
  177.8 0.0 copy-done.6
  177.8 12.5 %convolution_convert_fusion.1 = bf16[512,2048]{1,0:T(8,128)(2,1)} fusion(bf16[1280,2048]{1,0:T(8,128)(2,1)} %all-gather.15.cloned.1.call-done, bf16[512,2048]{1,0:T(8,128)(2,1)S(1)} %copy-done.6, bf16[2048,1280]{1,0:T(8,128)(2,1)} %all-gather.13.cloned.1.call-done, f32[512,1280]{1,0:T(8,128)} %fusion.22), kind=kOutput, calls=%fused_computation.5 | convolution fusion | flops 5373689856 | bytes 17301504 | tf_op jit(solution)/shard_map/dot_general | solution.py:45
  190.3 0.0 copy-start.1
  190.3 0.0 copy-start
  190.3 0.0 copy-start.2
  190.3 0.0 copy-start.3
  190.3 0.0 copy-start.4
  190.3 0.0 reduce-scatter.3.cloned.1.call-update
  190.3 0.0 all-gather.19.cloned.1.call-start
  190.4 0.5 all-gather.19.cloned.1.call-update
  190.9 0.0 all-gather.17.cloned.1.call-start
  190.9 0.4 copy-done.1
  191.3 0.2 fusion.5
  191.5 28.4 %reduce-scatter.3.cloned.1.call-done = bf16[128,2048]{1,0:T(8,128)(2,1)} async-done(((bf16[512,2048]{1,0:T(8,128)(2,1)}), bf16[128,2048]{1,0:T(8,128)(2,1)}) %reduce-scatter.3.cloned.1.call-update) | async-done | bytes 524304 | tf_op jit(solution)/shard_map/reduce_scatter | solution.py:19
  219.9 1.2 fusion.2
  221.2 0.0 copy-done
  221.2 0.0 copy-done.2
  221.2 0.0 copy-done.3
  221.2 1.6 fusion.15
  222.8 0.0 copy-done.4
  222.8 1.0 fusion.17
  223.8 0.0 all-gather.17.cloned.1.call-update
  223.8 0.0 all-gather.21.cloned.1.call-start
  223.9 0.7 all-gather.21.cloned.1.call-update
  224.6 0.0 all-gather.23.cloned.1.call-start
  224.6 0.7 all-gather.23.cloned.1.call-update
  225.3 0.2 reduce-scatter.5.cloned.1.call-start
  225.6 34.9 %all-gather.19.cloned.1.call-done = bf16[2048,1280]{1,0:T(8,128)(2,1)} async-done(((bf16[128,1280]{1,0:T(8,128)(2,1)}), bf16[2048,1280]{1,0:T(8,128)(2,1)}) %all-gather.19.cloned.1.call-update) | async-done | bytes 5242896 | tf_op jit(solution)/shard_map/all_gather | solution.py:12
  260.5 32.6 %all-gather.17.cloned.1.call-done = bf16[512,2048]{1,0:T(8,128)(2,1)} async-done(((bf16[128,2048]{1,0:T(8,128)(2,1)}), bf16[512,2048]{1,0:T(8,128)(2,1)}) %all-gather.17.cloned.1.call-update) | async-done | bytes 2097168 | tf_op jit(solution)/shard_map/all_gather | solution.py:30
  293.1 0.0 copy-start.7
  293.1 7.6 %fusion.23 = f32[512,1280]{1,0:T(8,128)} fusion(bf16[512,2048]{1,0:T(8,128)(2,1)} %all-gather.17.cloned.1.call-done, bf16[2048,1280]{1,0:T(8,128)(2,1)} %all-gather.19.cloned.1.call-done), kind=kOutput, calls=%fused_computation.43 | convolution fusion | flops 2684354560 | bytes 9961472 | tf_op jit(solution)/shard_map/dot_general | solution.py:35
  300.8 33.5 %all-gather.21.cloned.1.call-done = bf16[2048,1280]{1,0:T(8,128)(2,1)} async-done(((bf16[128,1280]{1,0:T(8,128)(2,1)}), bf16[2048,1280]{1,0:T(8,128)(2,1)}) %all-gather.21.cloned.1.call-update) | async-done | bytes 5242896 | tf_op jit(solution)/shard_map/all_gather | solution.py:12
  334.2 51.6 %all-gather.23.cloned.1.call-done = bf16[1280,2048]{1,0:T(8,128)(2,1)} async-done(((bf16[1280,128]{1,0:T(8,128)(2,1)}), bf16[1280,2048]{1,0:T(8,128)(2,1)}) %all-gather.23.cloned.1.call-update) | async-done | bytes 5242896 | tf_op jit(solution)/shard_map/all_gather | solution.py:40
  385.9 0.0 copy-done.7
  385.9 12.5 %convolution_convert_fusion = bf16[512,2048]{1,0:T(8,128)(2,1)} fusion(bf16[1280,2048]{1,0:T(8,128)(2,1)} %all-gather.23.cloned.1.call-done, bf16[512,2048]{1,0:T(8,128)(2,1)S(1)} %copy-done.7, bf16[2048,1280]{1,0:T(8,128)(2,1)} %all-gather.21.cloned.1.call-done, f32[512,1280]{1,0:T(8,128)} %fusion.23), kind=kOutput, calls=%fused_computation.4 | convolution fusion | flops 5373689856 | bytes 17301504 | tf_op jit(solution)/shard_map/dot_general | solution.py:45
  398.3 0.0 copy-start.5
  398.4 0.0 reduce-scatter.5.cloned.1.call-update
  398.4 29.6 %reduce-scatter.5.cloned.1.call-done = bf16[128,2048]{1,0:T(8,128)(2,1)} async-done(((bf16[512,2048]{1,0:T(8,128)(2,1)}), bf16[128,2048]{1,0:T(8,128)(2,1)}) %reduce-scatter.5.cloned.1.call-update) | async-done | bytes 524304 | tf_op jit(solution)/shard_map/reduce_scatter | solution.py:19
  428.0 1.2 fusion.9
  429.2 0.0 copy-done.5
  429.2 2.1 fusion.18
  (5 shorter events, 0.0 us)
Async XLA Ops:
  6.5 37.5 %all-gather.9.cloned.1.call-start = ((), (), s32[]{:S(2)}) async-start(), calls=%async_computation.2 | async-start | bytes 2621440 | tf_op jit(solution)/shard_map/all_gather | solution.py:30
  9.8 75.3 %all-gather.11.cloned.1.call-start = ((), (), s32[]{:S(2)}) async-start(), calls=%async_computation.3 | async-start | bytes 5570560 | tf_op jit(solution)/shard_map/all_gather | solution.py:12
  10.6 115.7 %all-gather.13.cloned.1.call-start = ((), (), s32[]{:S(2)}) async-start(), calls=%async_computation.4 | async-start | bytes 5570560 | tf_op jit(solution)/shard_map/all_gather | solution.py:12
  11.3 166.5 %all-gather.15.cloned.1.call-start = ((), (), s32[]{:S(2)}) async-start(), calls=%async_computation.5 | async-start | bytes 5570560 | tf_op jit(solution)/shard_map/all_gather | solution.py:40
  11.9 208.0 %reduce-scatter.3.cloned.1.call-start = ((), (), s32[]{:S(2)}) async-start(), calls=%async_computation.6 | async-start | bytes 2621440 | tf_op jit(solution)/shard_map/reduce_scatter | solution.py:19
  44.0 133.8 %copy-start.6 = (bf16[512,2048]{1,0:T(8,128)(2,1)S(1)}, bf16[512,2048]{1,0:T(8,128)(2,1)}, u32[]{:S(2)}) copy-start(bf16[512,2048]{1,0:T(8,128)(2,1)} %all-gather.9.cloned.1.call-done) | copy-start | bytes 6291460
  190.3 1.0 copy-start.1
  190.3 30.9 %copy-start = (bf16[128,2048]{1,0:T(8,128)(2,1)S(1)}, bf16[128,2048]{1,0:T(8,128)(2,1)}, u32[]{:S(2)}) copy-start(bf16[128,2048]{1,0:T(8,128)(2,1)} %param.13) | copy-start | bytes 1572868
  190.3 30.9 %copy-start.2 = (f32[2048]{0:T(1024)S(1)}, f32[2048]{0:T(1024)}, u32[]{:S(2)}) copy-start(f32[2048]{0:T(1024)} %param.20) | copy-start | bytes 24580
  190.3 30.9 %copy-start.3 = (f32[2048]{0:T(1024)S(1)}, f32[2048]{0:T(1024)}, u32[]{:S(2)}) copy-start(f32[2048]{0:T(1024)} %param.19) | copy-start | bytes 24580
  190.3 32.6 %copy-start.4 = (f32[2048]{0:T(1024)S(1)}, f32[2048]{0:T(1024)}, u32[]{:S(2)}) copy-start(f32[2048]{0:T(1024)} %param.21) | copy-start | bytes 24580
  190.3 70.2 %all-gather.19.cloned.1.call-start = ((), (), s32[]{:S(2)}) async-start(), calls=%async_computation.8 | async-start | bytes 5570560 | tf_op jit(solution)/shard_map/all_gather | solution.py:12
  190.9 102.2 %all-gather.17.cloned.1.call-start = ((), (), s32[]{:S(2)}) async-start(), calls=%async_computation.7 | async-start | bytes 2621440 | tf_op jit(solution)/shard_map/all_gather | solution.py:30
  223.8 110.4 %all-gather.21.cloned.1.call-start = ((), (), s32[]{:S(2)}) async-start(), calls=%async_computation.9 | async-start | bytes 5570560 | tf_op jit(solution)/shard_map/all_gather | solution.py:12
  224.6 161.2 %all-gather.23.cloned.1.call-start = ((), (), s32[]{:S(2)}) async-start(), calls=%async_computation.10 | async-start | bytes 5570560 | tf_op jit(solution)/shard_map/all_gather | solution.py:40
  225.3 202.7 %reduce-scatter.5.cloned.1.call-start = ((), (), s32[]{:S(2)}) async-start(), calls=%async_computation.11 | async-start | bytes 2621440 | tf_op jit(solution)/shard_map/reduce_scatter | solution.py:19
  293.1 92.7 %copy-start.7 = (bf16[512,2048]{1,0:T(8,128)(2,1)S(1)}, bf16[512,2048]{1,0:T(8,128)(2,1)}, u32[]{:S(2)}) copy-start(bf16[512,2048]{1,0:T(8,128)(2,1)} %all-gather.17.cloned.1.call-done) | copy-start | bytes 6291460
  398.3 30.9 %copy-start.5 = (f32[2048]{0:T(1024)S(1)}, f32[2048]{0:T(1024)}, u32[]{:S(2)}) copy-start(f32[2048]{0:T(1024)} %param.25) | copy-start | bytes 24580
Sparse Core Ops, SparseCore 0:
  9.9 34.0 all-gather.8
  45.7 39.3 all-gather.10
  86.8 39.4 all-gather.12
  127.8 49.9 all-gather.14
  190.4 29.4 reduce-scatter.2
  221.5 38.9 all-gather.18
  262.2 30.9 all-gather.16
  294.8 39.3 all-gather.20
  335.9 49.9 all-gather.22
  398.5 29.4 reduce-scatter.4
where the time goes:
time: 439 us; the launch traced here: 438 us
  waiting for transfers between devices  373 us (85%)
  matrix products  40.1 us (9%)
  between operations  13.6 us (3%)
  other arithmetic  10.7 us (2%)
    all_gather x4, waiting for transfers between devices, gathered(): return lax.all_gather(part, axis, axis=dim, tiled=True)  143 us
    all_gather x2, waiting for transfers between devices, half_branch(): down_block = lax.all_gather(down_piece, 'fs', axis=1, tiled=True)  103 us
    all_gather x2, waiting for transfers between devices, half_branch(): all_rows = lax.all_gather(normed, 'tp', axis=0, tiled=True)  64.7 us
    reduce_scatter x2, waiting for transfers between devices, own_rows(): lax.psum_scatter(everything.astype(jnp.bfloat16), axis, scatter_dimension...  58.1 us
    dot_general x2, matrix products, row_term(): return jnp.dot(rows, down_block, preferred_element_type=jnp.float32)  25 us
    dot_general x2, matrix products, add_rows(): gate_part = jnp.dot(columns, pieces[0], preferred_element_type=jnp.float32)  15.1 us
  transfers between devices with their start and end apart: 10, of which 10 were waited for; matrix products, arithmetic and copies ran while one was open for 4% of the time, Pallas kernels for 0%

commit v1 on v0

--- a/solution.py
+++ b/solution.py
@@ -4,6 +4,28 @@
 from jax.sharding import PartitionSpec as P
 
 epsilon = 1e-06
+
+
+def in_order(pieces, dim):
+    lengths = list(pieces.shape[1:])
+    lengths[dim] *= pieces.shape[0]
+    return jnp.moveaxis(pieces, 0, dim).reshape(lengths)
+
+
+def grow_blocks(shard, axis):
+    size = lax.axis_size(axis)
+    blocks = shard[None]
+    for level in range(size.bit_length() - 1):
+        bit = 1 << level
+        other = lax.ppermute(blocks, axis, [(i, i ^ bit) for i in range(size)])
+        both = jnp.stack([blocks, other])
+        upper = lax.axis_index(axis) >> level & 1
+        blocks = jnp.where(upper == 0, both, both[::-1]).reshape(-1, *shard.shape)
+    return blocks
+
+
+def collect(x, axis, dim):
+    return in_order(grow_blocks(x, axis), dim)
 
 
 def over_all(piece, axis, dim, step, start):
@@ -27,7 +49,7 @@
 
 
 def half_branch(normed, gate_piece, value_piece, down_piece):
-    all_rows = lax.all_gather(normed, "tp", axis=0, tiled=True)
+    all_rows = collect(normed, "tp", 0)
     empty = jnp.zeros((all_rows.shape[0], gate_piece.shape[1]), jnp.float32)
 
     def add_rows(totals, pieces, start):

time: 439 us -> 373 us (0.85)
  waiting for transfers between devices: 373 us -> 301 us
  starting transfers between devices: 0.54 us -> 7.53 us
    ppermute x0 -> x4, waiting for transfers between devices: none -> 70.3 us  [grow_blocks(): other = lax.ppermute(blocks, axis, [(i, i ^ bit) for i in range(size)])]
    all_gather x4, waiting for transfers between devices: 143 us -> 73.4 us  [gathered(): return lax.all_gather(part, axis, axis=dim, tiled=True)]
    all_gather x2 -> x0, waiting for transfers between devices: 64.7 us -> none  [half_branch(): all_rows = lax.all_gather(normed, 'tp', axis=0, tiled=True)]
    ppermute x0 -> x4, starting transfers between devices: none -> 7.26 us  [grow_blocks(): other = lax.ppermute(blocks, axis, [(i, i ^ bit) for i in range(size)])]
    all_gather x2, waiting for transfers between devices: 103 us -> 95.8 us  [half_branch(): down_block = lax.all_gather(down_piece, 'fs', axis=1, tiled=True)]
  transfers between devices with their start and end apart: 10 -> 12, of which waited for: 10 -> 10; matrix products, arithmetic and copies ran while one was open for 4% -> 6% of each run, Pallas kernels for 0% -> 0%
where the time goes in v1:
time: 373 us; the launch traced here: 372 us
  waiting for transfers between devices  301 us (81%)
  matrix products  38.7 us (10%)
  between operations  13.6 us (4%)
  other arithmetic  11.2 us (3%)
  starting transfers between devices  7.53 us (2%)
    all_gather x2, waiting for transfers between devices, half_branch(): down_block = lax.all_gather(down_piece, 'fs', axis=1, tiled=True)  95.8 us
    all_gather x4, waiting for transfers between devices, gathered(): return lax.all_gather(part, axis, axis=dim, tiled=True)  73.4 us
    ppermute x4, waiting for transfers between devices, grow_blocks(): other = lax.ppermute(blocks, axis, [(i, i ^ bit) for i in range(size)])  70.3 us
    reduce_scatter x2, waiting for transfers between devices, own_rows(): lax.psum_scatter(everything.astype(jnp.bfloat16), axis, scatter_dimension...  57.6 us
    dot_general x2, matrix products, row_term(): return jnp.dot(rows, down_block, preferred_element_type=jnp.float32)  25 us
    dot_general x2, matrix products, add_rows(): gate_part = jnp.dot(columns, pieces[0], preferred_element_type=jnp.float32)  13.7 us
  transfers between devices with their start and end apart: 12, of which 10 were waited for; matrix products, arithmetic and copies ran while one was open for 6% of the time, Pallas kernels for 0%

profile of v1, /device:TPU:1, one launch (start us, length us, event | category | flops | bytes accessed | tf_op | source)
XLA Modules:
  0.0 372.1 jit_solution(9268040958646858422)
XLA Ops:
  6.5 0.0 all-gather.7.cloned.1.call-start
  6.5 0.7 all-gather.7.cloned.1.call-update
  7.3 0.0 all-gather.11.cloned.1.call-start
  7.3 0.7 all-gather.11.cloned.1.call-update
  8.0 0.0 all-gather.9.cloned.1.call-start
  8.1 0.7 all-gather.9.cloned.1.call-update
  8.7 0.0 reduce-scatter.3.cloned.1.call-start
  8.8 1.2 fusion.12
  10.0 1.3 fusion.26
  11.3 2.5 collective-permute-start
  13.8 11.7 %collective-permute-done = bf16[1,128,2048]{2,1,0:T(8,128)(2,1)S(1)} collective-permute-done((bf16[1,128,2048]{2,1,0:T(8,128)(2,1)S(1)}, bf16[1,128,2048]{2,1,0:T(8,128)(2,1)S(1)}, u32[]{:S(2)}, u32[]{:S(2)}) %collective-permute-start) | collective-permute-done | bytes 524320 | tf_op jit(solution)/shard_map/ppermute | solution.py:20
  25.5 0.1 pad_maximum_fusion.2
  25.7 0.4 fusion.20
  26.1 3.2 collective-permute-start.1
  29.3 22.1 %collective-permute-done.1 = bf16[2,128,2048]{2,1,0:T(8,128)(2,1)S(1)} collective-permute-done((bf16[2,128,2048]{2,1,0:T(8,128)(2,1)S(1)}, bf16[2,128,2048]{2,1,0:T(8,128)(2,1)S(1)}, u32[]{:S(2)}, u32[]{:S(2)}) %collective-permute-start.1) | collective-permute-done | bytes 1048608 | tf_op jit(solution)/shard_map/ppermute | solution.py:20
  51.4 0.2 pad_maximum_fusion
  51.6 0.5 reverse_select_fusion.1
  52.1 0.0 all-gather.7.cloned.1.call-done
  52.1 6.9 %fusion.30 = f32[512,1280]{1,0:T(8,128)} fusion(bf16[512,2048]{1,0:T(8,128)(2,1)S(1)} %bitcast.42, bf16[2048,1280]{1,0:T(8,128)(2,1)} %all-gather.7.cloned.1.call-done), kind=kOutput, calls=%fused_computation.58 | convolution fusion | flops 2684354560 | bytes 9961472 | tf_op jit(solution)/shard_map/dot_general | solution.py:57
  59.0 44.2 %all-gather.11.cloned.1.call-done = bf16[1280,2048]{1,0:T(8,128)(2,1)} async-done(((bf16[1280,128]{1,0:T(8,128)(2,1)}), bf16[1280,2048]{1,0:T(8,128)(2,1)}) %all-gather.11.cloned.1.call-update) | async-done | bytes 5242896 | tf_op jit(solution)/shard_map/all_gather | solution.py:62
  103.2 40.7 %all-gather.9.cloned.1.call-done = bf16[2048,1280]{1,0:T(8,128)(2,1)} async-done(((bf16[128,1280]{1,0:T(8,128)(2,1)}), bf16[2048,1280]{1,0:T(8,128)(2,1)}) %all-gather.9.cloned.1.call-update) | async-done | bytes 5242896 | tf_op jit(solution)/shard_map/all_gather | solution.py:34
  143.9 12.5 %convolution_convert_fusion.1 = bf16[512,2048]{1,0:T(8,128)(2,1)} fusion(bf16[1280,2048]{1,0:T(8,128)(2,1)} %all-gather.11.cloned.1.call-done, bf16[512,2048]{1,0:T(8,128)(2,1)S(1)} %bitcast.43, bf16[2048,1280]{1,0:T(8,128)(2,1)} %all-gather.9.cloned.1.call-done, f32[512,1280]{1,0:T(8,128)} %fusion.30), kind=kOutput, calls=%fused_computation.7 | convolution fusion | flops 5373689856 | bytes 17301504 | tf_op jit(solution)/shard_map/dot_general | solution.py:67
  156.4 0.0 copy-start.1
  156.4 0.0 copy-start
  156.4 0.0 copy-start.2
  156.4 0.0 copy-start.3
  156.4 0.0 copy-start.4
  156.4 0.0 reduce-scatter.3.cloned.1.call-update
  156.4 0.0 all-gather.13.cloned.1.call-start
  156.5 0.5 all-gather.13.cloned.1.call-update
  157.0 0.0 all-gather.15.cloned.1.call-start
  157.0 0.5 all-gather.15.cloned.1.call-update
  157.6 0.0 all-gather.17.cloned.1.call-start
  157.6 0.7 all-gather.17.cloned.1.call-update
  158.3 0.0 reduce-scatter.5.cloned.1.call-start
  158.4 0.0 copy-done.1
  158.4 0.2 fusion.5
  158.6 28.0 %reduce-scatter.3.cloned.1.call-done = bf16[128,2048]{1,0:T(8,128)(2,1)} async-done(((bf16[512,2048]{1,0:T(8,128)(2,1)}), bf16[128,2048]{1,0:T(8,128)(2,1)}) %reduce-scatter.3.cloned.1.call-update) | async-done | bytes 524304 | tf_op jit(solution)/shard_map/reduce_scatter | solution.py:41
  186.6 1.2 fusion.2
  187.8 0.0 copy-done
  187.8 0.0 copy-done.2
  187.8 0.0 copy-done.3
  187.8 1.6 fusion.15
  189.5 0.0 copy-done.4
  189.5 0.2 fusion.24
  189.7 0.1 collective-permute-start.2
  189.8 12.8 %collective-permute-done.2 = bf16[1,128,2048]{2,1,0:T(8,128)(2,1)S(1)} collective-permute-done((bf16[1,128,2048]{2,1,0:T(8,128)(2,1)S(1)}, bf16[1,128,2048]{2,1,0:T(8,128)(2,1)S(1)}, u32[]{:S(2)}, u32[]{:S(2)}) %collective-permute-start.2) | collective-permute-done | bytes 524320 | tf_op jit(solution)/shard_map/ppermute | solution.py:20
  202.6 0.1 pad_maximum_fusion.3
  202.7 0.2 fusion.22
  202.9 1.4 collective-permute-start.3
  204.3 23.6 %collective-permute-done.3 = bf16[2,128,2048]{2,1,0:T(8,128)(2,1)S(1)} collective-permute-done((bf16[2,128,2048]{2,1,0:T(8,128)(2,1)S(1)}, bf16[2,128,2048]{2,1,0:T(8,128)(2,1)S(1)}, u32[]{:S(2)}, u32[]{:S(2)}) %collective-permute-start.3) | collective-permute-done | bytes 1048608 | tf_op jit(solution)/shard_map/ppermute | solution.py:20
  227.9 0.2 pad_maximum_fusion.1
  228.1 0.5 reverse_select_fusion
  228.6 0.0 all-gather.13.cloned.1.call-done
  228.6 6.9 %fusion.31 = f32[512,1280]{1,0:T(8,128)} fusion(bf16[512,2048]{1,0:T(8,128)(2,1)S(1)} %bitcast.40, bf16[2048,1280]{1,0:T(8,128)(2,1)} %all-gather.13.cloned.1.call-done), kind=kOutput, calls=%fused_computation.59 | convolution fusion | flops 2684354560 | bytes 9961472 | tf_op jit(solution)/shard_map/dot_general | solution.py:57
  235.5 32.7 %all-gather.15.cloned.1.call-done = bf16[2048,1280]{1,0:T(8,128)(2,1)} async-done(((bf16[128,1280]{1,0:T(8,128)(2,1)}), bf16[2048,1280]{1,0:T(8,128)(2,1)}) %all-gather.15.cloned.1.call-update) | async-done | bytes 5242896 | tf_op jit(solution)/shard_map/all_gather | solution.py:34
  268.2 51.6 %all-gather.17.cloned.1.call-done = bf16[1280,2048]{1,0:T(8,128)(2,1)} async-done(((bf16[1280,128]{1,0:T(8,128)(2,1)}), bf16[1280,2048]{1,0:T(8,128)(2,1)}) %all-gather.17.cloned.1.call-update) | async-done | bytes 5242896 | tf_op jit(solution)/shard_map/all_gather | solution.py:62
  319.8 12.5 %convolution_convert_fusion = bf16[512,2048]{1,0:T(8,128)(2,1)} fusion(bf16[1280,2048]{1,0:T(8,128)(2,1)} %all-gather.17.cloned.1.call-done, bf16[512,2048]{1,0:T(8,128)(2,1)S(1)} %bitcast.41, bf16[2048,1280]{1,0:T(8,128)(2,1)} %all-gather.15.cloned.1.call-done, f32[512,1280]{1,0:T(8,128)} %fusion.31), kind=kOutput, calls=%fused_computation.6 | convolution fusion | flops 5373689856 | bytes 17301504 | tf_op jit(solution)/shard_map/dot_general | solution.py:67
  332.2 0.0 copy-start.5
  332.2 0.0 reduce-scatter.5.cloned.1.call-update
  332.3 29.6 %reduce-scatter.5.cloned.1.call-done = bf16[128,2048]{1,0:T(8,128)(2,1)} async-done(((bf16[512,2048]{1,0:T(8,128)(2,1)}), bf16[128,2048]{1,0:T(8,128)(2,1)}) %reduce-scatter.5.cloned.1.call-update) | async-done | bytes 524304 | tf_op jit(solution)/shard_map/reduce_scatter | solution.py:41
  361.9 1.2 fusion.9
  363.1 0.0 copy-done.5
  363.1 2.1 fusion.18
  (5 shorter events, 0.0 us)
Async XLA Ops:
  6.5 45.6 %all-gather.7.cloned.1.call-start = ((), (), s32[]{:S(2)}) async-start(), calls=%async_computation.2 | async-start | bytes 5570560 | tf_op jit(solution)/shard_map/all_gather | solution.py:34
  7.3 95.9 %all-gather.11.cloned.1.call-start = ((), (), s32[]{:S(2)}) async-start(), calls=%async_computation.4 | async-start | bytes 5570560 | tf_op jit(solution)/shard_map/all_gather | solution.py:62
  8.0 135.9 %all-gather.9.cloned.1.call-start = ((), (), s32[]{:S(2)}) async-start(), calls=%async_computation.3 | async-start | bytes 5570560 | tf_op jit(solution)/shard_map/all_gather | solution.py:34
  8.7 177.8 %reduce-scatter.3.cloned.1.call-start = ((), (), s32[]{:S(2)}) async-start(), calls=%async_computation.5 | async-start | bytes 2621440 | tf_op jit(solution)/shard_map/reduce_scatter | solution.py:41
  11.3 14.3 %collective-permute-start = (bf16[1,128,2048]{2,1,0:T(8,128)(2,1)S(1)}, bf16[1,128,2048]{2,1,0:T(8,128)(2,1)S(1)}, u32[]{:S(2)}, u32[]{:S(2)}) collective-permute-start(bf16[1,128,2048]{2,1,0:T(8,128)(2,1)S(1)} %get-tuple-element.14), channel_id=1, source_target_pairs={{0,1},{1,0},{2,3},{3,2},{4,5},{5,4},{6,7},{7,6},{8,9},{9,8},{10,11... | collective-permute-start | bytes 1572872 | tf_op jit(solution)/shard_map/ppermute | solution.py:20
  26.1 25.3 %collective-permute-start.1 = (bf16[2,128,2048]{2,1,0:T(8,128)(2,1)S(1)}, bf16[2,128,2048]{2,1,0:T(8,128)(2,1)S(1)}, u32[]{:S(2)}, u32[]{:S(2)}) collective-permute-start(bf16[2,128,2048]{2,1,0:T(8,128)(2,1)S(1)} %get-tuple-element.10), channel_id=1, source_target_pairs={{0,2},{1,3},{2,0},{3,1},{4,6},{5,7},{6,4},{7,5},{8,10},{9,11},{10,... | collective-permute-start | bytes 3145736 | tf_op jit(solution)/shard_map/ppermute | solution.py:20
  156.4 2.0 copy-start.1
  156.4 31.4 %copy-start = (bf16[128,2048]{1,0:T(8,128)(2,1)S(1)}, bf16[128,2048]{1,0:T(8,128)(2,1)}, u32[]{:S(2)}) copy-start(bf16[128,2048]{1,0:T(8,128)(2,1)} %param.13) | copy-start | bytes 1572868
  156.4 31.4 %copy-start.2 = (f32[2048]{0:T(1024)S(1)}, f32[2048]{0:T(1024)}, u32[]{:S(2)}) copy-start(f32[2048]{0:T(1024)} %param.20) | copy-start | bytes 24580
  156.4 31.5 %copy-start.3 = (f32[2048]{0:T(1024)S(1)}, f32[2048]{0:T(1024)}, u32[]{:S(2)}) copy-start(f32[2048]{0:T(1024)} %param.19) | copy-start | bytes 24580
  156.4 33.1 %copy-start.4 = (f32[2048]{0:T(1024)S(1)}, f32[2048]{0:T(1024)}, u32[]{:S(2)}) copy-start(f32[2048]{0:T(1024)} %param.21) | copy-start | bytes 24580
  156.4 72.2 %all-gather.13.cloned.1.call-start = ((), (), s32[]{:S(2)}) async-start(), calls=%async_computation.6 | async-start | bytes 5570560 | tf_op jit(solution)/shard_map/all_gather | solution.py:34
  157.0 111.2 %all-gather.15.cloned.1.call-start = ((), (), s32[]{:S(2)}) async-start(), calls=%async_computation.7 | async-start | bytes 5570560 | tf_op jit(solution)/shard_map/all_gather | solution.py:34
  157.6 162.2 %all-gather.17.cloned.1.call-start = ((), (), s32[]{:S(2)}) async-start(), calls=%async_computation.8 | async-start | bytes 5570560 | tf_op jit(solution)/shard_map/all_gather | solution.py:62
  158.3 203.6 %reduce-scatter.5.cloned.1.call-start = ((), (), s32[]{:S(2)}) async-start(), calls=%async_computation.9 | async-start | bytes 2621440 | tf_op jit(solution)/shard_map/reduce_scatter | solution.py:41
  189.7 12.9 %collective-permute-start.2 = (bf16[1,128,2048]{2,1,0:T(8,128)(2,1)S(1)}, bf16[1,128,2048]{2,1,0:T(8,128)(2,1)S(1)}, u32[]{:S(2)}, u32[]{:S(2)}) collective-permute-start(bf16[1,128,2048]{2,1,0:T(8,128)(2,1)S(1)} %get-tuple-element.12), channel_id=1, source_target_pairs={{0,1},{1,0},{2,3},{3,2},{4,5},{5,4},{6,7},{7,6},{8,9},{9,8},{10,11... | collective-permute-start | bytes 1572872 | tf_op jit(solution)/shard_map/ppermute | solution.py:20
  202.9 25.0 %collective-permute-start.3 = (bf16[2,128,2048]{2,1,0:T(8,128)(2,1)S(1)}, bf16[2,128,2048]{2,1,0:T(8,128)(2,1)S(1)}, u32[]{:S(2)}, u32[]{:S(2)}) collective-permute-start(bf16[2,128,2048]{2,1,0:T(8,128)(2,1)S(1)} %get-tuple-element.8), channel_id=1, source_target_pairs={{0,2},{1,3},{2,0},{3,1},{4,6},{5,7},{6,4},{7,5},{8,10},{9,11},{10,... | collective-permute-start | bytes 3145736 | tf_op jit(solution)/shard_map/ppermute | solution.py:20
  332.2 30.9 %copy-start.5 = (f32[2048]{0:T(1024)S(1)}, f32[2048]{0:T(1024)}, u32[]{:S(2)}) copy-start(f32[2048]{0:T(1024)} %param.25) | copy-start | bytes 24580
Sparse Core Ops, SparseCore 0:
  9.0 42.5 all-gather.6
  53.2 49.9 all-gather.10
  104.9 38.9 all-gather.8
  156.5 29.9 reduce-scatter.2
  188.1 39.1 all-gather.12
  228.9 39.2 all-gather.14
  269.8 49.9 all-gather.16
  332.4 29.4 reduce-scatter.4
